TPU v7x, 32 devices: a whole 2x2x4 slice. The times are simulated.
32 devices in a mesh: sp: 8 (over z, y), tp: 4 (over x, core).
Axes of the slice: x: 2, y: 2, z: 4, core: 2. Of those that a mesh axis runs over, the one named last changes fastest.
Arguments:
- tokens: bfloat16 [1024, 2048], P('sp', 'tp'), may hold values from -28 to 28
- norm_gain: bfloat16 [1, 2048], P(None, 'tp'), may hold values from 0.099609375 to 1.8984375
- conv_b_w: bfloat16 [2048, 1024], P(None, 'tp'), may hold values from -0.125 to 0.125
- conv_c_w: bfloat16 [2048, 1024], P(None, 'tp'), may hold values from -0.125 to 0.125
- conv_u_w: bfloat16 [2048, 1024], P(None, 'tp'), may hold values from -0.125 to 0.125
- conv_taps: bfloat16 [3, 1024], P(None, 'tp'), may hold values from -3.5 to 3.5
- query_w: bfloat16 [2048, 2048], P(None, 'tp'), may hold values from -0.125 to 0.125
- key_w: bfloat16 [2048, 2048], P(None, 'tp'), may hold values from -0.125 to 0.125
- value_w: bfloat16 [2048, 2048], P(None, 'tp'), may hold values from -0.125 to 0.125
- outgate_w: bfloat16 [2048, 2048], P(None, 'tp'), may hold values from -0.125 to 0.125
- gate_w: bfloat16 [2048, 2, 8], P(None, None, 'tp'), may hold values from -0.125 to 0.125
- gate_bias: float32 [2, 8], P(None, 'tp'), may hold values from -5 to 150
- mem_gain: bfloat16 [2048], P('tp'), may hold values from 0.099609375 to 1.8984375
- conv_out_w: bfloat16 [1024, 2048], P('tp'), may hold values from -0.1875 to 0.1875
- mem_out_w: bfloat16 [2048, 2048], P('tp'), may hold values from -0.125 to 0.125
Outputs:
- layer_out: bfloat16 [1024, 2048], P(('sp', 'tp'))
All inputs are finite; a program needn't handle non-finite values.
Results may differ from a plain program's by a relative error of at most 0.014.
The roundings to bfloat16 on the way count: a program that leaves them out, or rounds other values in their place, can miss the bound.
Values may be sent and summed in bfloat16 or wider, within the bound.
A program may use at most 64 MiB of HBM per device.

v0:
```python
import jax
import jax.numpy as jnp
from jax import lax
from jax.sharding import PartitionSpec as P

HEAD_DIM = 256
BLOCK = 128
MDIM = 2048
EPS = 1e-06
LOWEST = -1e30
HIGH = lax.Precision.HIGHEST


def shifted(value, axis, by):
    count = lax.axis_size(axis)
    pairs = [(i, i + by) for i in range(count) if 0 <= i + by < count]
    return lax.ppermute(value, axis, pairs)


def prefix(value, axis, join, neutral):
    count, mine = (lax.axis_size(axis), lax.axis_index(axis))
    pieces = jax.tree.map(lambda part: lax.all_gather(part, axis), value)
    total = jax.tree.map(
        lambda part, zero: jnp.full_like(part, 0) + jnp.asarray(zero, part.dtype), value, neutral
    )

    def prefix_step(position, total):
        longer = join(total, jax.tree.map(lambda part: part[position], pieces))
        return jax.tree.map(lambda new, old: jnp.where(position < mine, new, old), longer, total)

    return lax.fori_loop(0, count - 1, prefix_step, total)


def local_pass(queries, keys, values, input_pre, log_forget):
    count, width = queries.shape
    blocks = count // BLOCK

    def local_step(carry, inputs):
        memory, normer, stabil, decay_sum = carry
        query_block, key_block, value_block, input_gate, forget_block = inputs
        causal = jnp.tril(jnp.ones((BLOCK, BLOCK), dtype=bool))
        running = jnp.cumsum(forget_block)
        decays = jnp.where(
            causal, running[:, None] - running[None, :] + input_gate[None, :], -jnp.inf
        )
        inter = running + stabil
        row_max = jnp.maximum(inter, jnp.max(decays, axis=1))
        weights = jnp.exp(decays - row_max[:, None])
        scores = jnp.dot(query_block, key_block.T, precision=HIGH) * weights
        carried = jnp.exp(inter - row_max)
        numer_part = carried[:, None] * jnp.dot(query_block, memory, precision=HIGH) + jnp.dot(
            scores, value_block, precision=HIGH
        )
        denom_part = carried * jnp.dot(query_block, normer, precision=HIGH) + jnp.sum(
            scores, axis=1
        )
        new_stabil = row_max[-1]
        key_weight = jnp.exp(running[-1] - running + input_gate - new_stabil)
        fade = jnp.exp(running[-1] + stabil - new_stabil)
        memory = fade * memory + jnp.dot(
            (key_weight[:, None] * key_block).T, value_block, precision=HIGH
        )
        normer = fade * normer + jnp.dot(key_weight, key_block, precision=HIGH)
        outputs = (numer_part, denom_part, row_max, decay_sum + running)
        return ((memory, normer, new_stabil, decay_sum + running[-1]), outputs)

    inputs = (
        queries.reshape(blocks, BLOCK, width),
        keys.reshape(blocks, BLOCK, width),
        values.reshape(blocks, BLOCK, width),
        input_pre.reshape(blocks, BLOCK),
        log_forget.reshape(blocks, BLOCK),
    )
    start = (
        jnp.zeros((width, width), jnp.float32),
        jnp.zeros((width,), jnp.float32),
        jnp.zeros((), jnp.float32),
        jnp.zeros((), jnp.float32),
    )
    final, rows = lax.scan(local_step, start, inputs)
    memory, normer, stabil, decay_sum = final
    numer_rows, denom_rows, row_max, row_decay = rows
    return (
        numer_rows.reshape(count, width),
        denom_rows.reshape(count),
        row_max.reshape(count),
        row_decay.reshape(count),
        decay_sum,
        stabil,
        memory,
        normer,
    )


def finish(queries, numer_rows, denom_rows, row_max, row_decay, stabil_in, memory_in, normer_in):
    from_before = jnp.dot(queries, memory_in, precision=HIGH)
    normer_before = jnp.dot(queries, normer_in, precision=HIGH)
    top = jnp.maximum(row_max, row_decay + stabil_in)
    own_scale = jnp.exp(row_max - top)
    past_scale = jnp.exp(row_decay + stabil_in - top)
    numer_all = own_scale[:, None] * numer_rows + past_scale[:, None] * from_before
    denom_all = own_scale * denom_rows + past_scale * normer_before
    return numer_all / jnp.maximum(jnp.abs(denom_all), jnp.exp(-top))[:, None]


def join_state(earlier, later):
    sum_early, stab_early, mem_early, norm_early = earlier[:4]
    sum_late, stab_late, mem_late, norm_late = later[:4]
    top = jnp.maximum(sum_late + stab_early, stab_late)
    early_scale = jnp.exp(sum_late + stab_early - top)
    late_scale = jnp.exp(stab_late - top)
    joined = (
        sum_early + sum_late,
        top,
        early_scale[:, None, None] * mem_early + late_scale[:, None, None] * mem_late,
        early_scale[:, None] * norm_early + late_scale[:, None] * norm_late,
    )
    if len(earlier) > 4:
        edge = jnp.where(later[5][0] > 0, later[4], earlier[4])
        joined = joined + (edge, jnp.maximum(earlier[5], later[5]))
    return joined


def body(
    tokens,
    norm_gain,
    conv_b_w,
    conv_c_w,
    conv_u_w,
    conv_taps,
    query_w,
    key_w,
    value_w,
    outgate_w,
    gate_w,
    gate_bias,
    mem_gain,
    conv_out_w,
    mem_out_w,
):
    count = tokens.shape[0]
    model = conv_b_w.shape[0]
    weights = (
        conv_b_w,
        conv_c_w,
        conv_u_w,
        query_w,
        key_w,
        value_w,
        outgate_w,
        gate_w.reshape(model, -1),
    )
    piece = lax.all_gather(tokens, "tp", axis=1, tiled=True)
    gain_piece = lax.all_gather(norm_gain, "tp", axis=1, tiled=True)
    wide = piece.astype(jnp.float32)
    scaled = (wide * gain_piece.astype(jnp.float32)).astype(jnp.bfloat16)
    squares = jnp.sum(wide * wide, axis=1)
    totals = tuple(
        (jnp.dot(scaled, weight, preferred_element_type=jnp.float32) for weight in weights)
    )
    folded = (squares,) + totals
    inv_rms = lax.rsqrt(folded[0] / model + EPS)[:, None]

    def project(total):
        return lax.optimization_barrier((inv_rms * total).astype(jnp.bfloat16)).astype(jnp.float32)

    gate_b, gate_c, gate_u, queries, keys, values, outgate = [
        project(total) for total in folded[1:8]
    ]
    heads = gate_bias.shape[1]
    gates = inv_rms * folded[8]
    input_pre = gates[:, :heads] + gate_bias[0]
    forget_pre = gates[:, heads:] + gate_bias[1]
    mixed_in = (gate_c * gate_u).astype(jnp.bfloat16)
    reach = conv_taps.shape[0] - 1
    head_q = queries.reshape(count, heads, HEAD_DIM)
    head_k = keys.reshape(count, heads, HEAD_DIM) * HEAD_DIM ** (-0.5)
    head_v = values.reshape(count, heads, HEAD_DIM)
    local = jax.vmap(local_pass, in_axes=1, out_axes=(1, 1, 1, 1, 0, 0, 0, 0))(
        head_q, head_k, head_v, input_pre, jax.nn.log_sigmoid(forget_pre)
    )
    numer_rows, denom_rows, row_max, row_decay, decay_sum, stabil, memory, normer = local
    identity = (
        jnp.zeros((heads,), jnp.float32),
        jnp.full((heads,), LOWEST, jnp.float32),
        jnp.zeros((heads, HEAD_DIM, HEAD_DIM), jnp.float32),
        jnp.zeros((heads, HEAD_DIM), jnp.float32),
    )
    before = shifted(mixed_in[count - reach :], "sp", 1)
    incoming = prefix((decay_sum, stabil, memory, normer), "sp", join_state, identity)
    padded = jnp.concatenate([before, mixed_in], axis=0).astype(jnp.float32)
    taps = conv_taps.astype(jnp.float32)
    conv_sum = taps[0] * padded[0:count]
    for offset in range(1, reach + 1):
        conv_sum = conv_sum + taps[offset] * padded[offset : offset + count]
    y_conv = (gate_b * conv_sum).astype(jnp.bfloat16)
    mem_raw = jax.vmap(finish, in_axes=(1, 1, 1, 1, 1, 0, 0, 0), out_axes=1)(
        head_q, numer_rows, denom_rows, row_max, row_decay, incoming[1], incoming[2], incoming[3]
    )
    flat_raw = mem_raw.reshape(count, -1)
    own_squares = jnp.sum(flat_raw * flat_raw, axis=1)
    all_squares = lax.psum(own_squares, "tp")
    mem_norm = flat_raw * lax.rsqrt(all_squares / MDIM + EPS)[:, None]
    mem_norm = mem_norm * mem_gain.astype(jnp.float32)[None, :]
    y_mem = (jax.nn.sigmoid(outgate) * mem_norm).astype(jnp.bfloat16)
    return lax.psum_scatter(
        (
            jnp.dot(y_conv, conv_out_w, preferred_element_type=jnp.float32)
            + jnp.dot(y_mem, mem_out_w, preferred_element_type=jnp.float32)
        ).astype(jnp.bfloat16),
        "tp",
        scatter_dimension=0,
        tiled=True,
    )


def solution(mesh):
    return jax.shard_map(
        body,
        mesh=mesh,
        in_specs=(
            P("sp", "tp"),
            P(None, "tp"),
            P(None, "tp"),
            P(None, "tp"),
            P(None, "tp"),
            P(None, "tp"),
            P(None, "tp"),
            P(None, "tp"),
            P(None, "tp"),
            P(None, "tp"),
            P(None, None, "tp"),
            P(None, "tp"),
            P("tp"),
            P("tp", None),
            P("tp", None),
        ),
        out_specs=P(("sp", "tp"), None),
        check_vma=False,
    )
```

profile of v0, /device:TPU:0, one launch (start us, length us, event | category | flops | bytes accessed | tf_op | source)
XLA Modules:
  0.0 148.9 jit_solution(2480114630991469454)
XLA Ops:
  6.6 0.8 slice_bitcast_fusion
  7.4 6.3 %all_gather.31 = bf16[1,2048]{1,0:T(2,128)(2,1)S(1)} all-gather(bf16[1,512]{1,0:T(2,128)(2,1)} %param.18), channel_id=1, replica_groups=mesh['sp'=8,'tp'=4] {'tp'}, dimensions={1}, use_global_device_ids=true | all-gather | bytes 5120 | tf_op jit(solution)/shard_map/all_gather | solution.py:154
  13.7 0.7 reshape.140
  14.5 7.9 %all_gather.30 = bf16[128,2048]{1,0:T(8,128)(2,1)S(1)} all-gather(bf16[128,512]{1,0:T(8,128)(2,1)} %param.17), channel_id=1, replica_groups=mesh['sp'=8,'tp'=4] {'tp'}, dimensions={1}, use_global_device_ids=true | all-gather | bytes 655360 | tf_op jit(solution)/shard_map/all_gather | solution.py:153
  22.9 0.3 reduce_window_sum.14
  23.7 2.2 %fusion.15 = bf16[128,512]{1,0:T(8,128)(2,1)S(1)} fusion(bf16[2048,512]{1,0:T(8,128)(2,1)} %param.24, f32[128]{0:T(128)S(1)} %add_rsqrt_fusion.1, bf16[128,2048]{1,0:T(8,128)(2,1)S(1)} %all_gather.30, f32[2048]{0:T(1024)S(1)} %bitcast.213), kind=kOutput, calls=%fused_computation.34 | convolution fusion | flops 269352960 | bytes 2761216 | tf_op jit(solution)/shard_map/dot_general | solution.py:159
  25.9 0.4 fusion.16
  26.4 1.3 convolution_add_fusion.1
  27.7 1.5 %fusion.19 = bf16[128,256]{1,0:T(8,128)(2,1)S(1)} fusion(bf16[2048,256]{1,0:T(8,128)(2,1)} %param.20, f32[128]{0:T(128)S(1)} %add_rsqrt_fusion.1, bf16[128,2048]{1,0:T(8,128)(2,1)S(1)} %all_gather.30, f32[2048]{0:T(1024)S(1)} %bitcast.215), kind=kOutput, calls=%fused_computation.42 | convolution fusion | flops 135069696 | bytes 1647104 | tf_op jit(solution)/shard_map/dot_general | solution.py:159
  29.3 1.5 %fusion.20 = bf16[128,256]{1,0:T(8,128)(2,1)S(1)} fusion(bf16[2048,256]{1,0:T(8,128)(2,1)} %param.21, f32[128]{0:T(128)S(1)} %add_rsqrt_fusion.1, bf16[128,2048]{1,0:T(8,128)(2,1)S(1)} %all_gather.30, f32[2048]{0:T(1024)S(1)} %bitcast.216), kind=kOutput, calls=%fused_computation.43 | convolution fusion | flops 135069696 | bytes 1647104 | tf_op jit(solution)/shard_map/dot_general | solution.py:159
  30.9 3.5 %collective-permute-start = (bf16[2,256]{1,0:T(2,128)(2,1)S(1)}, bf16[2,256]{1,0:T(2,128)(2,1)S(1)}, u32[]{:S(2)}, u32[]{:S(2)}) collective-permute-start(bf16[2,256]{1,0:T(2,128)(2,1)S(1)} %slice.57), channel_id=1, source_target_pairs={{0,4},{4,8},{8,12},{12,16},{16,20},{20,24},{24,28},{1,5},{5,9},{9,... | collective-permute-start | bytes 3080 | tf_op jit(solution)/shard_map/ppermute | solution.py:17
  34.4 0.6 dynamic-slice.10
  36.1 2.3 %fusion.17 = bf16[128,512]{1,0:T(8,128)(2,1)S(1)} fusion(bf16[2048,512]{1,0:T(8,128)(2,1)} %param.23, f32[128]{0:T(128)S(1)} %add_rsqrt_fusion.1, bf16[128,2048]{1,0:T(8,128)(2,1)S(1)} %all_gather.30, f32[2048]{0:T(1024)S(1)} %bitcast.217), kind=kOutput, calls=%fused_computation.36 | convolution fusion | flops 269352960 | bytes 2761216 | tf_op jit(solution)/shard_map/dot_general | solution.py:159
  38.9 0.3 fusion.80
  39.3 0.3 convolution_bitcast_fusion.2
  40.0 0.4 fusion.14
  40.5 27.0 %all-gather.4 = f32[8,2,256]{2,1,0:T(2,128)S(1)} all-gather(f32[1,2,256]{2,1,0:T(2,128)S(1)} %fusion.63), channel_id=5, replica_groups=mesh['sp'=8,'tp'=4] {'sp'}, dimensions={0}, use_global_device_ids=true | all-gather | bytes 18432 | tf_op jit(solution)/shard_map/all_gather | solution.py:22
  67.5 19.8 %all-reduce.2 = (f32[16]{0:T(128)S(1)}, f32[16]{0:T(128)S(1)}) all-reduce(f32[16]{0:T(128)S(1)} %dynamic-update-slice, f32[16]{0:T(128)S(1)} %dynamic-update-slice.1), channel_id=2, replica_groups=mesh['sp'=8,'tp'=4] {'sp'}, use_global_device_ids=true, to_apply=%add | all-reduce | flops 32 | bytes 256
  87.5 2.5 %fusion.50 = f32[128,2048]{1,0:T(8,128)} fusion(bf16[256,2048]{1,0:T(8,128)(2,1)} %param.30, f32[130,256]{1,0:T(8,128)S(1)} %maximum_convert_fusion, bf16[128,256]{1,0:T(8,128)(2,1)S(1)} %fusion.18, f32[256]{0:T(256)S(1)} %bitcast.230, f32[256]{0:T(256)S(1)} %bitcast.229, f32[256]{0:T(256)S(1)} %bitcast.228), kind=kOutput, calls=%fused_computation.85 | convolution fusion | flops 134479872 | bytes 2558976 | tf_op jit(solution)/shard_map/dot_general | solution.py:208
  90.1 12.7 %all-gather.7.cloned.1.call-done = f32[16,256,256]{2,1,0:T(8,128)} async-done(((f32[2,256,256]{2,1,0:T(8,128)}), f32[16,256,256]{2,1,0:T(8,128)}) %all-gather.7.cloned.1.call-update) | async-done | bytes 4194320 | tf_op jit(solution)/shard_map/all_gather | solution.py:22
  102.8 9.3 %while.5 = (s32[]{:T(128)}, f32[2]{0:T(128)S(1)}, f32[2,256,256]{2,1,0:T(8,128)S(1)}, f32[2,256]{1,0:T(2,128)S(1)}, s32[]{:T(128)}, /*index=5*/f32[8,2]{1,0:T(8,...) while((s32[]{:T(128)}, f32[2]{0:T(128)S(1)}, ...), condition=%wide.region_4.5_spmd.clone, body=%wide.region_3.4_spmd.clone.sunk | while | flops 657940 | bytes 1579278 | solution.py:31
  102.9 1.2 fusion.96
  104.3 1.2 fusion.96
  105.6 1.2 fusion.96
  106.9 1.2 fusion.96
  108.3 1.2 fusion.96
  109.6 1.2 fusion.96
  111.0 1.2 fusion.96
  112.7 0.5 multiply_reduce_fusion
  113.2 5.7 %psum.7 = f32[128]{0:T(128)S(1)} all-reduce(f32[128]{0:T(128)S(1)} %get-tuple-element.276), channel_id=1, replica_groups=mesh['sp'=8,'tp'=4] {'tp'}, use_global_device_ids=true, to_apply=%region_7.8 | all-reduce | flops 128 | bytes 1024 | tf_op jit(solution)/shard_map/psum | solution.py:202
  118.9 2.5 %fusion.7 = bf16[128,2048]{1,0:T(8,128)(2,1)} fusion(f32[128,2048]{1,0:T(8,128)} %fusion.50, bf16[512,2048]{1,0:T(8,128)(2,1)S(1)} %copy-done, f32[128,512]{1,0:T(8,128)S(1)} %bitcast.211, bf16[128,512]{1,0:T(8,128)(2,1)S(1)} %fusion.14, f32[512]{0:T(512)S(1)} %convert_element_type.84, f32[128]{0:T(128)S(1)} %add_rsqrt_fusion), kind=kOutput, calls=%fused_computation.16 | convolution fusion | flops 269484032 | bytes 4065792 | tf_op jit(solution)/shard_map/dot_general | solution.py:209
  121.4 20.7 %reduce-scatter.2.cloned.1.call-done = bf16[32,2048]{1,0:T(8,128)(2,1)} async-done(((bf16[128,2048]{1,0:T(8,128)(2,1)}), bf16[32,2048]{1,0:T(8,128)(2,1)}) %reduce-scatter.2.cloned.1.call-update) | async-done | bytes 131088 | tf_op jit(solution)/shard_map/reduce_scatter | solution.py:206
  (75 shorter events, 4.2 us)
Async XLA Ops:
  6.5 112.4 %copy-start = (bf16[512,2048]{1,0:T(8,128)(2,1)S(1)}, bf16[512,2048]{1,0:T(8,128)(2,1)}, u32[]{:S(2)}) copy-start(bf16[512,2048]{1,0:T(8,128)(2,1)} %param.31) | copy-start | bytes 6291460
  6.5 96.3 %all-gather.7.cloned.1.call-start = ((), (), s32[]{:S(2)}) async-start(), calls=%async_computation.2 | async-start | bytes 4718592 | tf_op jit(solution)/shard_map/all_gather | solution.py:22
  23.2 2.7 %copy-start.1 = (bf16[2048,512]{1,0:T(8,128)(2,1)S(1)}, bf16[2048,512]{1,0:T(8,128)(2,1)}, u32[]{:S(2)}) copy-start(bf16[2048,512]{1,0:T(8,128)(2,1)} %param.25) | copy-start | bytes 6291460
  27.7 6.8 %copy-start.6 = (u32[32]{0:T(128)S(1)}, u32[32]{0:T(128)}, u32[]{:S(2)}) copy-start(u32[32]{0:T(128)} %constant.86) | copy-start | bytes 388
  27.7 114.4 %reduce-scatter.2.cloned.1.call-start = ((), (), s32[]{:S(2)}) async-start(), calls=%async_computation.1 | async-start | bytes 655360 | tf_op jit(solution)/shard_map/reduce_scatter | solution.py:206
  29.3 9.5 %copy-start.4 = (bf16[3,256]{1,0:T(4,128)(2,1)S(1)}, bf16[3,256]{1,0:T(4,128)(2,1)}, u32[]{:S(2)}) copy-start(bf16[3,256]{1,0:T(4,128)(2,1)} %param.22) | copy-start | bytes 4612
  30.9 56.6 %collective-permute-start = (bf16[2,256]{1,0:T(2,128)(2,1)S(1)}, bf16[2,256]{1,0:T(2,128)(2,1)S(1)}, u32[]{:S(2)}, u32[]{:S(2)}) collective-permute-start(bf16[2,256]{1,0:T(2,128)(2,1)S(1)} %slice.57), channel_id=1, source_target_pairs={{0,4},{4,8},{8,12},{12,16},{16,20},{20,24},{24,28},{1,5},{5,9},{9,... | collective-permute-start | bytes 3080 | tf_op jit(solution)/shard_map/ppermute | solution.py:17
  36.1 3.5 %copy-start.3 = (bf16[2048,256]{1,0:T(8,128)(2,1)S(1)}, bf16[2048,256]{1,0:T(8,128)(2,1)}, u32[]{:S(2)}) copy-start(bf16[2048,256]{1,0:T(8,128)(2,1)} %param.19) | copy-start | bytes 3145732
  38.4 1.6 %copy-start.2 = (bf16[2048,512]{1,0:T(8,128)(2,1)S(1)}, bf16[2048,512]{1,0:T(8,128)(2,1)}, u32[]{:S(2)}) copy-start(bf16[2048,512]{1,0:T(8,128)(2,1)} %param.26) | copy-start | bytes 6291460
  39.6 47.7 %copy-start.5 = (bf16[512]{0:T(512)(128)(2,1)S(1)}, bf16[512]{0:T(512)(128)(2,1)}, u32[]{:S(2)}) copy-start(bf16[512]{0:T(512)(128)(2,1)} %param.29) | copy-start | bytes 3076
Sparse Core Ops, SparseCore 0:
  27.8 74.9 all-gather.6
  121.6 20.4 reduce-scatter.1
where the time goes:
time: 150 us; the launch traced here: 149 us
  blocking collectives  66.7 us (44%)
  waiting for transfers between devices  33.4 us (22%)
  matrix products  17.4 us (12%)
  between operations  14.3 us (10%)
  other arithmetic  10.4 us (7%)
  starting transfers between devices  3.57 us (2%)
  local copies, waits for them, and re-layouts  2.92 us (2%)
    all_gather x1, blocking collectives, prefix(): pieces = jax.tree.map(lambda part: lax.all_gather(part, axis), value)  27 us
    reduce_scatter x1, waiting for transfers between devices, body(): lax.psum_scatter((jnp.dot(y_conv, conv_out_w, preferred_element_type=jnp....  20.7 us
    unnamed x1, blocking collectives  19.8 us
    all_gather x1, waiting for transfers between devices, prefix(): pieces = jax.tree.map(lambda part: lax.all_gather(part, axis), value)  12.7 us
    dot_general x8, matrix products, body(): jnp.dot(scaled, weight, preferred_element_type=jnp.float32)  9 us
    select_n x14, other arithmetic, prefix_step(): jnp.where(position < mine, new, old)  8.88 us
    all_gather x1, blocking collectives, body(): piece = lax.all_gather(tokens, 'tp', axis=1, tiled=True)  7.85 us
    all_gather x1, blocking collectives, body(): gain_piece = lax.all_gather(norm_gain, 'tp', axis=1, tiled=True)  6.32 us
  transfers between devices with their start and end apart: 3, of which 2 were waited for; matrix products, arithmetic and copies ran while one was open for 7% of the time, Pallas kernels for 0%

commit v1 on v0

--- a/solution.py
+++ b/solution.py
@@ -150,7 +150,10 @@
         outgate_w,
         gate_w.reshape(model, -1),
     )
-    piece = lax.all_gather(tokens, "tp", axis=1, tiled=True)
+    size = lax.axis_size("tp")
+    tiles = jnp.stack([tokens for _ in range(size)])
+    tiles = lax.all_to_all(tiles, "tp", split_axis=0, concat_axis=0)
+    piece = jnp.concatenate(tiles, axis=1)
     gain_piece = lax.all_gather(norm_gain, "tp", axis=1, tiled=True)
     wide = piece.astype(jnp.float32)
     scaled = (wide * gain_piece.astype(jnp.float32)).astype(jnp.bfloat16)

time: 150 us -> 154 us (1.027)
  waiting for transfers between devices: 33.4 us -> 23.9 us
  local copies, waits for them, and re-layouts: 2.92 us -> 11.2 us
  starting transfers between devices: 3.57 us -> 9.06 us
  blocking collectives: 66.7 us -> 61.6 us
  other arithmetic: 10.4 us -> 13.5 us
    all_gather x1, waiting for transfers between devices: 12.7 us -> 3.31 us  [prefix(): pieces = jax.tree.map(lambda part: lax.all_gather(part, axis), value)]
    all_gather x1 -> x0, blocking collectives: 7.85 us -> none  [body(): piece = lax.all_gather(tokens, 'tp', axis=1, tiled=True)]
    unnamed x19 -> x68, local copies, waits for them, and re-layouts: 1.15 us -> 6.67 us
    all_to_all x0 -> x1, starting transfers between devices: none -> 4.24 us  [body(): tiles = lax.all_to_all(tiles, 'tp', split_axis=0, concat_axis=0)]
    all_gather x1, blocking collectives: 6.32 us -> 9.79 us  [body(): gain_piece = lax.all_gather(norm_gain, 'tp', axis=1, tiled=True)]
  transfers between devices with their start and end apart: 3 -> 4, of which waited for: 2 -> 2; matrix products, arithmetic and copies ran while one was open for 7% -> 14% of each run, Pallas kernels for 0% -> 0%
where the time goes in v1:
time: 154 us; the launch traced here: 153 us
  blocking collectives  61.6 us (40%)
  waiting for transfers between devices  23.9 us (16%)
  matrix products  18.4 us (12%)
  between operations  14.6 us (9%)
  other arithmetic  13.5 us (9%)
  local copies, waits for them, and re-layouts  11.2 us (7%)
  starting transfers between devices  9.06 us (6%)
    all_gather x1, blocking collectives, prefix(): pieces = jax.tree.map(lambda part: lax.all_gather(part, axis), value)  26.9 us
    reduce_scatter x1, waiting for transfers between devices, body(): lax.psum_scatter((jnp.dot(y_conv, conv_out_w, preferred_element_type=jnp....  20.6 us
    unnamed x1, blocking collectives  19.3 us
    all_gather x1, blocking collectives, body(): gain_piece = lax.all_gather(norm_gain, 'tp', axis=1, tiled=True)  9.79 us
    dot_general x8, matrix products, body(): jnp.dot(scaled, weight, preferred_element_type=jnp.float32)  8.93 us
    select_n x14, other arithmetic, prefix_step(): jnp.where(position < mine, new, old)  8.88 us
    unnamed x68, local copies, waits for them, and re-layouts  6.67 us
    psum x1, blocking collectives, body(): all_squares = lax.psum(own_squares, 'tp')  5.66 us
  transfers between devices with their start and end apart: 4, of which 2 were waited for; matrix products, arithmetic and copies ran while one was open for 14% of the time, Pallas kernels for 0%

profile of v1, /device:TPU:0, one launch (start us, length us, event | category | flops | bytes accessed | tf_op | source)
XLA Modules:
  0.0 152.7 jit_solution(1333496649463170908)
XLA Ops:
  6.5 1.2 copy.31
  7.7 0.9 stack.2
  8.6 4.2 %all-to-all-start = ((bf16[4,128,512]{1,2,0:T(8,128)(2,1)}), bf16[4,128,512]{1,2,0:T(8,128)(2,1)S(1)}, u32[]{:S(2)}, u32[]{:S(2)}) async-start(bf16[4,128,512]{1,2,0:T(8,128)(2,1)} %stack.2), calls=%async_computation | async-start | bytes 1048576 | tf_op jit(solution)/shard_map/all_to_all | solution.py:155
  12.8 9.8 %all_gather.27 = bf16[1,2048]{1,0:T(2,128)(2,1)S(1)} all-gather(bf16[1,512]{1,0:T(2,128)(2,1)} %param.18), channel_id=1, replica_groups=mesh['sp'=8,'tp'=4] {'tp'}, dimensions={1}, use_global_device_ids=true | all-gather | bytes 5120 | tf_op jit(solution)/shard_map/all_gather | solution.py:157
  26.9 2.2 %fusion.15 = bf16[128,512]{1,0:T(8,128)(2,1)S(1)} fusion(bf16[128,2048]{0,1:T(8,128)(2,1)S(1)} %fusion.21, bf16[2048,512]{1,0:T(8,128)(2,1)} %param.24, f32[128]{0:T(128)S(1)} %add_rsqrt_fusion.1), kind=kOutput, calls=%fused_computation.32 | convolution fusion | flops 268566528 | bytes 2753024 | tf_op jit(solution)/shard_map/dot_general | solution.py:162
  29.2 1.1 fusion.16
  30.4 1.3 convolution_add_fusion.1
  31.8 1.3 convert_element_type.112
  33.1 1.3 dynamic-slice.10
  35.1 1.4 fusion.70
  37.0 1.2 dynamic-update-slice
  38.8 1.3 dynamic-update-slice.1
  40.1 1.8 %fusion.19 = bf16[128,256]{1,0:T(8,128)(2,1)S(1)} fusion(bf16[128,2048]{0,1:T(8,128)(2,1)S(1)} %fusion.21, bf16[2048,256]{1,0:T(8,128)(2,1)} %param.20, f32[128]{0:T(128)} %copy-done.13), kind=kOutput, calls=%fused_computation.40 | convolution fusion | flops 134283264 | bytes 1638912 | tf_op jit(solution)/shard_map/dot_general | solution.py:162
  42.0 1.6 %fusion.20 = bf16[128,256]{1,0:T(8,128)(2,1)S(1)} fusion(bf16[128,2048]{0,1:T(8,128)(2,1)S(1)} %fusion.21, bf16[2048,256]{1,0:T(8,128)(2,1)} %param.21, f32[128]{0:T(128)} %copy-done.13), kind=kOutput, calls=%fused_computation.41 | convolution fusion | flops 134283264 | bytes 1638912 | tf_op jit(solution)/shard_map/dot_general | solution.py:162
  44.3 4.8 %collective-permute-start = (bf16[2,256]{1,0:T(2,128)(2,1)}, bf16[2,256]{1,0:T(2,128)(2,1)}, u32[]{:S(2)}, u32[]{:S(2)}) collective-permute-start(bf16[2,256]{1,0:T(2,128)(2,1)} %slice.57), channel_id=1, source_target_pairs={{0,4},{4,8},{8,12},{12,16},{16,20},{20,24},{24,28},{1,5},{5,9},{9,... | collective-permute-start | bytes 3080 | tf_op jit(solution)/shard_map/ppermute | solution.py:17
  51.9 1.0 fusion.18
  53.4 26.9 %all-gather.4 = f32[8,2,256]{2,1,0:T(2,128)S(1)} all-gather(f32[1,2,256]{2,1,0:T(2,128)S(1)} %fusion.54), channel_id=5, replica_groups=mesh['sp'=8,'tp'=4] {'sp'}, dimensions={0}, use_global_device_ids=true | all-gather | bytes 18432 | tf_op jit(solution)/shard_map/all_gather | solution.py:22
  80.3 19.3 %all-reduce.2 = (f32[16]{0:T(128)S(1)}, f32[16]{0:T(128)S(1)}) all-reduce(f32[16]{0:T(128)} %dynamic-update-slice, f32[16]{0:T(128)} %dynamic-update-slice.1), channel_id=2, replica_groups=mesh['sp'=8,'tp'=4] {'sp'}, use_global_device_ids=true, to_apply=%add | all-reduce | flops 32 | bytes 256
  99.7 0.9 maximum_convert_fusion
  100.6 2.6 %fusion.49 = f32[128,2048]{1,0:T(8,128)} fusion(bf16[256,2048]{1,0:T(8,128)(2,1)} %param.30, f32[130,256]{1,0:T(8,128)S(1)} %maximum_convert_fusion, bf16[128,256]{1,0:T(8,128)(2,1)} %fusion.18, f32[256]{0:T(256)} %bitcast.241, f32[256]{0:T(256)S(1)} %bitcast.240, f32[256]{0:T(256)S(1)} %bitcast.239), kind=kOutput, calls=%fused_computation.85 | convolution fusion | flops 134479872 | bytes 2558976 | tf_op jit(solution)/shard_map/dot_general | solution.py:211
  103.2 3.3 %all-gather.7.cloned.1.call-done = f32[16,256,256]{2,1,0:T(8,128)} async-done(((f32[2,256,256]{2,1,0:T(8,128)}), f32[16,256,256]{2,1,0:T(8,128)}) %all-gather.7.cloned.1.call-update) | async-done | bytes 4194320 | tf_op jit(solution)/shard_map/all_gather | solution.py:22
  106.6 9.4 %while.5 = (s32[]{:T(128)}, f32[2]{0:T(128)S(1)}, f32[2,256,256]{2,1,0:T(8,128)S(1)}, f32[2,256]{1,0:T(2,128)S(1)}, s32[]{:T(128)}, /*index=5*/f32[8,2]{1,0:T(8,...) while((s32[]{:T(128)}, f32[2]{0:T(128)S(1)}, ...), condition=%wide.region_4.5_spmd.clone, body=%wide.region_3.4_spmd.clone.sunk | while | flops 657940 | bytes 1579278 | solution.py:31
  106.7 1.2 fusion.95
  108.0 1.2 fusion.95
  109.4 1.2 fusion.95
  110.7 1.2 fusion.95
  112.1 1.2 fusion.95
  113.4 1.2 fusion.95
  114.7 1.2 fusion.95
  117.0 5.7 %psum.7 = f32[128]{0:T(128)S(1)} all-reduce(f32[128]{0:T(128)S(1)} %get-tuple-element.278), channel_id=1, replica_groups=mesh['sp'=8,'tp'=4] {'tp'}, use_global_device_ids=true, to_apply=%region_7.8 | all-reduce | flops 128 | bytes 1024 | tf_op jit(solution)/shard_map/psum | solution.py:205
  122.7 2.5 %fusion.7 = bf16[128,2048]{1,0:T(8,128)(2,1)} fusion(f32[128,2048]{1,0:T(8,128)} %fusion.49, bf16[512,2048]{1,0:T(8,128)(2,1)S(1)} %copy-done, f32[128,512]{1,0:T(8,128)S(1)} %bitcast.229, bf16[128,512]{1,0:T(8,128)(2,1)S(1)} %fusion.14, f32[512]{0:T(512)S(1)} %copy-done.21, f32[128]{0:T(128)S(1)} %add_rsqrt_fusion), kind=kOutput, calls=%fused_computation.16 | convolution fusion | flops 269484032 | bytes 4065792 | tf_op jit(solution)/shard_map/dot_general | solution.py:212
  125.3 20.6 %reduce-scatter.2.cloned.1.call-done = bf16[32,2048]{1,0:T(8,128)(2,1)} async-done(((bf16[128,2048]{1,0:T(8,128)(2,1)}), bf16[32,2048]{1,0:T(8,128)(2,1)}) %reduce-scatter.2.cloned.1.call-update) | async-done | bytes 131088 | tf_op jit(solution)/shard_map/reduce_scatter | solution.py:209
  (129 shorter events, 11.4 us)
Async XLA Ops:
  6.5 116.2 %copy-start = (bf16[512,2048]{1,0:T(8,128)(2,1)S(1)}, bf16[512,2048]{1,0:T(8,128)(2,1)}, u32[]{:S(2)}) copy-start(bf16[512,2048]{1,0:T(8,128)(2,1)} %param.31) | copy-start | bytes 6291460
  8.6 15.6 %all-to-all-start = ((bf16[4,128,512]{1,2,0:T(8,128)(2,1)}), bf16[4,128,512]{1,2,0:T(8,128)(2,1)S(1)}, u32[]{:S(2)}, u32[]{:S(2)}) async-start(bf16[4,128,512]{1,2,0:T(8,128)(2,1)} %stack.2), calls=%async_computation | async-start | bytes 1048576 | tf_op jit(solution)/shard_map/all_to_all | solution.py:155
  12.8 93.7 %all-gather.7.cloned.1.call-start = ((), (), s32[]{:S(2)}) async-start(), calls=%async_computation.3 | async-start | bytes 4718592 | tf_op jit(solution)/shard_map/all_gather | solution.py:22
  24.6 2.4 %copy-start.13 = (f32[128]{0:T(128)}, f32[128]{0:T(128)S(1)}, u32[]{:S(2)}) copy-start(f32[128]{0:T(128)S(1)} %add_rsqrt_fusion.1) | copy-start | bytes 1540
  24.8 1.3 copy-start.17
  25.2 1.0 copy-start.10
  25.3 0.9 copy-start.15
  25.3 0.8 copy-start.24
  26.2 4.2 %copy-start.19 = (f32[2,128]{1,0:T(2,128)}, f32[2,128]{1,0:T(2,128)S(1)}, u32[]{:S(2)}) copy-start(f32[2,128]{1,0:T(2,128)S(1)} %subtract_exponential_fusion.4) | copy-start | bytes 3076
  26.6 2.6 %copy-start.1 = (bf16[2048,512]{1,0:T(8,128)(2,1)S(1)}, bf16[2048,512]{1,0:T(8,128)(2,1)}, u32[]{:S(2)}) copy-start(bf16[2048,512]{1,0:T(8,128)(2,1)} %param.25) | copy-start | bytes 6291460
  31.7 114.1 %reduce-scatter.2.cloned.1.call-start = ((), (), s32[]{:S(2)}) async-start(), calls=%async_computation.2 | async-start | bytes 655360 | tf_op jit(solution)/shard_map/reduce_scatter | solution.py:209
  40.1 8.9 %copy-start.2 = (bf16[2048,512]{1,0:T(8,128)(2,1)S(1)}, bf16[2048,512]{1,0:T(8,128)(2,1)}, u32[]{:S(2)}) copy-start(bf16[2048,512]{1,0:T(8,128)(2,1)} %param.23) | copy-start | bytes 6291460
  40.1 8.9 %copy-start.14 = (f32[128]{0:T(128)S(1)}, f32[128]{0:T(128)}, u32[]{:S(2)}) copy-start(f32[128]{0:T(128)} %copy-done.13) | copy-start | bytes 1540
  42.0 7.6 %copy-start.20 = (f32[2,128]{1,0:T(2,128)S(1)}, f32[2,128]{1,0:T(2,128)}, u32[]{:S(2)}) copy-start(f32[2,128]{1,0:T(2,128)} %copy-done.19) | copy-start | bytes 3076
  42.0 7.8 %copy-start.26 = (f32[2]{0:T(128)S(1)}, f32[2]{0:T(128)}, u32[]{:S(2)}) copy-start(f32[2]{0:T(128)} %get-tuple-element.236) | copy-start | bytes 28
  43.6 7.1 %copy-start.11 = (f32[2,128]{1,0:T(2,128)S(1)}, f32[2,128]{1,0:T(2,128)}, u32[]{:S(2)}) copy-start(f32[2,128]{1,0:T(2,128)} %copy-done.10) | copy-start | bytes 3076
  43.6 7.1 %copy-start.18 = (f32[2,128]{1,0:T(2,128)S(1)}, f32[2,128]{1,0:T(2,128)}, u32[]{:S(2)}) copy-start(f32[2,128]{1,0:T(2,128)} %copy-done.17) | copy-start | bytes 3076
  43.6 7.1 %copy-start.25 = (f32[2,128]{1,0:T(2,128)S(1)}, f32[2,128]{1,0:T(2,128)}, u32[]{:S(2)}) copy-start(f32[2,128]{1,0:T(2,128)} %copy-done.24) | copy-start | bytes 3076
  44.3 7.6 %copy-start.4 = (bf16[2048,256]{1,0:T(8,128)(2,1)S(1)}, bf16[2048,256]{1,0:T(8,128)(2,1)}, u32[]{:S(2)}) copy-start(bf16[2048,256]{1,0:T(8,128)(2,1)} %param.19) | copy-start | bytes 3145732
  44.3 55.4 %collective-permute-start = (bf16[2,256]{1,0:T(2,128)(2,1)}, bf16[2,256]{1,0:T(2,128)(2,1)}, u32[]{:S(2)}, u32[]{:S(2)}) collective-permute-start(bf16[2,256]{1,0:T(2,128)(2,1)} %slice.57), channel_id=1, source_target_pairs={{0,4},{4,8},{8,12},{12,16},{16,20},{20,24},{24,28},{1,5},{5,9},{9,... | collective-permute-start | bytes 3080 | tf_op jit(solution)/shard_map/ppermute | solution.py:17
  49.5 3.8 %copy-start.5 = (bf16[128,512]{1,0:T(8,128)(2,1)}, bf16[128,512]{1,0:T(8,128)(2,1)S(1)}, u32[]{:S(2)}) copy-start(bf16[128,512]{1,0:T(8,128)(2,1)S(1)} %fusion.17) | copy-start | bytes 393220
  49.6 3.3 %copy-start.3 = (bf16[2048,512]{1,0:T(8,128)(2,1)S(1)}, bf16[2048,512]{1,0:T(8,128)(2,1)}, u32[]{:S(2)}) copy-start(bf16[2048,512]{1,0:T(8,128)(2,1)} %param.26) | copy-start | bytes 6291460
  51.8 48.7 %copy-start.22 = (f32[1,256]{1,0:T(1,128)S(1)}, f32[1,256]{1,0:T(1,128)}, u32[]{:S(2)}) copy-start(f32[1,256]{1,0:T(1,128)} %get-tuple-element.271) | copy-start | bytes 3076
  51.9 48.7 %copy-start.23 = (f32[1,256]{1,0:T(1,128)S(1)}, f32[1,256]{1,0:T(1,128)}, u32[]{:S(2)}) copy-start(f32[1,256]{1,0:T(1,128)} %get-tuple-element.272) | copy-start | bytes 3076
  52.9 53.6 %copy-start.8 = (f32[2]{0:T(128)S(1)}, f32[2]{0:T(128)}, u32[]{:S(2)}) copy-start(f32[2]{0:T(128)} %custom-call) | copy-start | bytes 28
  52.9 53.6 %copy-start.9 = (f32[2,256]{1,0:T(2,128)S(1)}, f32[2,256]{1,0:T(2,128)}, u32[]{:S(2)}) copy-start(f32[2,256]{1,0:T(2,128)} %custom-call.2) | copy-start | bytes 6148
  106.5 9.4 %copy-start.6 = (bf16[128,512]{1,0:T(8,128)(2,1)S(1)}, bf16[128,512]{1,0:T(8,128)(2,1)}, u32[]{:S(2)}) copy-start(bf16[128,512]{1,0:T(8,128)(2,1)} %copy-done.5) | copy-start | bytes 393220
  106.5 9.6 %copy-start.12 = (f32[2,128]{1,0:T(2,128)S(1)}, f32[2,128]{1,0:T(2,128)}, u32[]{:S(2)}) copy-start(f32[2,128]{1,0:T(2,128)} %copy-done.10) | copy-start | bytes 3076
  106.5 9.6 %copy-start.16 = (f32[2,128]{1,0:T(2,128)S(1)}, f32[2,128]{1,0:T(2,128)}, u32[]{:S(2)}) copy-start(f32[2,128]{1,0:T(2,128)} %copy-done.15) | copy-start | bytes 3076
  106.5 9.6 %copy-start.29 = (f32[2,1,128]{2,1,0:T(1,128)S(1)}, f32[2,1,128]{2,1,0:T(1,128)}, u32[]{:S(2)}) copy-start(f32[2,1,128]{2,1,0:T(1,128)} %fusion.32) | copy-start | bytes 3076
  106.6 9.6 %copy-start.30 = (f32[2,128]{1,0:T(2,128)S(1)}, f32[2,128]{1,0:T(2,128)}, u32[]{:S(2)}) copy-start(f32[2,128]{1,0:T(2,128)} %get-tuple-element.276) | copy-start | bytes 3076
  115.9 6.8 %copy-start.21 = (f32[512]{0:T(512)S(1)}, f32[512]{0:T(512)}, u32[]{:S(2)}) copy-start(f32[512]{0:T(512)} %convert_element_type.112) | copy-start | bytes 6148
  (3 other events, 1.7 us)
Sparse Core Ops, SparseCore 0:
  31.8 74.6 all-gather.6
  125.4 20.4 reduce-scatter.1
